TPU v7x, 128 devices: a whole 4x4x4 slice. The times are simulated.
128 devices in a mesh: ep: 64 (over z, y, x), tp: 2 (over core).
Axes of the slice: x: 4, y: 4, z: 4, core: 2. Of those that a mesh axis runs over, the one named last changes fastest.
Arguments:
- inputs: bfloat16 [1024, 2048], P('ep'), may hold values from -6 to 6
- positions: int32 [1024], P('ep'), may hold values from 1024 to 8191
- ret_state: float32 [1024, 12, 128, 128], P('ep', 'tp'), may hold values from -4 to 4
- norm_mix: bfloat16 [2048], replicated, may hold values from 0.099609375 to 1.8984375
- w_query: bfloat16 [2048, 1536], P('ep', 'tp'), may hold values from -0.375 to 0.375
- w_key: bfloat16 [2048, 1536], P('ep', 'tp'), may hold values from -0.375 to 0.375
- w_value: bfloat16 [2048, 1536], P('ep', 'tp'), may hold values from -0.375 to 0.375
- w_gate_in: bfloat16 [2048, 1536], P('ep', 'tp'), may hold values from -0.375 to 0.375
- head_gain: bfloat16 [1536], P('tp'), may hold values from 0.099609375 to 1.8984375
- w_out: bfloat16 [1536, 2048], P('tp', 'ep'), may hold values from -0.15625 to 0.15625
- norm_ffn: bfloat16 [2048], replicated, may hold values from 0.099609375 to 1.8984375
- route_ids: int32 [1024, 4], P('ep'), may hold values from 0 to 63, all different within a row; in each aligned block of 16 rows (0 to 15, 16 to 31, ...) at most 2 rows name the same one
- route_weight: bfloat16 [1024, 4], P('ep'), may hold values from 0.19921875 to 1
- exp_gate: bfloat16 [64, 2048, 1024], P('ep', None, 'tp'), may hold values from -0.125 to 0.125
- exp_up: bfloat16 [64, 2048, 1024], P('ep', None, 'tp'), may hold values from -0.125 to 0.125
- exp_down: bfloat16 [64, 1024, 2048], P('ep', 'tp'), may hold values from -0.1875 to 0.1875
- dense_gate: bfloat16 [2048, 4096], P(None, ('ep', 'tp')), may hold values from -0.125 to 0.125
- dense_up: bfloat16 [2048, 4096], P(None, ('ep', 'tp')), may hold values from -0.125 to 0.125
- dense_down: bfloat16 [4096, 2048], P(('ep', 'tp')), may hold values from -0.375 to 0.375
- branch_gate: bfloat16 [2048], replicated, may hold values from -0.125 to 0.125
Outputs:
- layer_out: bfloat16 [1024, 2048], P('ep')
- new_state: float32 [1024, 12, 128, 128], P('ep', 'tp')
Inputs may be any that keep to these rules, and one draw needn't show every extreme that they name: `route_ids`: each row names 4 different experts. Among the rows of one index of ep no expert is named more than 2 times, a bound that some block reaches.
All inputs are finite; a program needn't handle non-finite values.
Results may differ from a plain program's by a relative error of at most 0.015.
Values may be sent and summed in bfloat16 or wider, within the bound.
A program may use at most 128 MiB of HBM per device.

v0:
```python
import jax
import jax.numpy as jnp
from jax import lax
from jax.sharding import PartitionSpec as P

D = 2048
HEADS = 12


EPS = 1e-06


def in_one_piece(arrays, axis, dim, along):
    both = jnp.concatenate(arrays, axis=along)
    out, at, done = (lax.all_gather(both, axis, axis=dim, tiled=True), 0, [])
    for a in arrays:
        done.append(lax.slice_in_dim(out, at, at + a.shape[along], axis=along))
        at += a.shape[along]
    return tuple(done)


def sent_to_all(array, axis):
    copies = jnp.broadcast_to(array, (lax.axis_size(axis), *array.shape))
    return lax.all_to_all(copies, axis, split_axis=0, concat_axis=0, tiled=True)


def over_copies(array, axis):
    everything = sent_to_all(array, axis)
    return jnp.sum(everything.astype(jnp.float32), axis=0)


def split_up(array, dim, size):
    before, after = (array.shape[:dim], array.shape[dim + 1 :])
    return jnp.moveaxis(array.reshape(*before, size, -1, *after), dim, 0)


def summed_on_arrival(array, axis, dim):
    size = lax.axis_size(axis)
    tiles = lax.all_to_all(split_up(array, dim, size), axis, 0, 0, tiled=True)
    return jnp.sum(tiles.astype(jnp.float32), axis=0)


def rms_scale(values, scales):
    widened = values.astype(jnp.float32)
    scaled = widened * lax.rsqrt(jnp.mean(widened * widened, axis=-1, keepdims=True) + EPS)
    return (scaled * scales.astype(jnp.float32)).astype(jnp.bfloat16)


def rotary_angles(positions, head_dim):
    halfway = head_dim // 2
    frequency = 10000.0 ** (-jnp.arange(halfway, dtype=jnp.float32) * 2.0 / head_dim)
    return positions.astype(jnp.float32)[:, None] * frequency[None, :]


def rotate_heads(values, angles):
    halfway = values.shape[-1] // 2
    cosine = jnp.cos(angles)[:, None, :]
    sine_of = jnp.sin(angles)[:, None, :]
    leading = values[..., :halfway]
    trailing = values[..., halfway:]
    return jnp.concatenate(
        [leading * cosine - trailing * sine_of, trailing * cosine + leading * sine_of], axis=-1
    )


def log_decay(head_count):
    spread = jnp.arange(head_count, dtype=jnp.float32) * (5.0 / max(head_count - 1, 1))
    return jnp.log1p(-(2.0 ** (-5.0 - spread)))


def retain(queries, keys_in, values_in, gate_pre, old_state, positions, scales, log_gamma):
    row_count, head_count, head_dim = (old_state.shape[0], old_state.shape[1], old_state.shape[2])
    angles = rotary_angles(positions, head_dim)
    rot_query = rotate_heads(
        queries.astype(jnp.float32).reshape(row_count, head_count, head_dim), angles
    )
    rot_key = rotate_heads(
        keys_in.astype(jnp.float32).reshape(row_count, head_count, head_dim), angles
    ) * head_dim ** (-0.5)
    value_heads = values_in.astype(jnp.float32).reshape(row_count, head_count, head_dim)
    new_state = (
        jnp.exp(log_gamma)[None, :, None, None] * old_state
        + rot_key[:, :, :, None] * value_heads[:, :, None, :]
    )
    readout = jnp.einsum("shd,shdv->shv", rot_query, new_state, precision=lax.Precision.HIGHEST)
    centred = readout - jnp.mean(readout, axis=-1, keepdims=True)
    normed = centred * lax.rsqrt(jnp.mean(centred * centred, axis=-1, keepdims=True) + EPS)
    normed = normed * scales.astype(jnp.float32).reshape(head_count, head_dim)
    gated_out = normed.reshape(row_count, head_count * head_dim) * jax.nn.silu(
        gate_pre.astype(jnp.float32)
    )
    return (gated_out.astype(jnp.bfloat16), new_state)


def slot_of(route_ids, expert_count, capacity):
    flat_ids = route_ids.reshape(-1)
    onehot = (flat_ids[:, None] == jnp.arange(expert_count, dtype=jnp.int32)[None, :]).astype(
        jnp.int32
    )
    ranking = jnp.sum((jnp.cumsum(onehot, axis=0) - 1) * onehot, axis=1)
    return flat_ids * capacity + ranking


def on_device(
    inputs,
    positions,
    ret_state,
    norm_mix,
    w_query,
    w_key,
    w_value,
    w_gate_in,
    head_gain,
    w_out,
    norm_ffn,
    route_ids,
    route_weight,
    exp_gate,
    exp_up,
    exp_down,
    dense_gate,
    dense_up,
    dense_down,
    branch_gate,
):
    seq_count = inputs.shape[0]
    top_count = route_ids.shape[1]
    ep_size = lax.axis_size("ep")
    local_experts = exp_gate.shape[0]
    expert_count = ep_size * local_experts
    capacity = max(2, 2 * seq_count * top_count // expert_count)
    normed = rms_scale(inputs, norm_mix)
    segments = in_one_piece((w_query, w_key, w_value, w_gate_in), "ep", 0, 1)
    totals = tuple(
        (
            jnp.dot(normed, weight_rows, preferred_element_type=jnp.float32)
            for weight_rows in segments
        )
    )
    queries, keys_new, values_new, gate_pre = [member.astype(jnp.bfloat16) for member in totals]
    local_heads = ret_state.shape[1]
    log_gamma = lax.dynamic_slice_in_dim(
        log_decay(HEADS), lax.axis_index("tp") * local_heads, local_heads
    )
    retained, new_state = retain(
        queries, keys_new, values_new, gate_pre, ret_state, positions, head_gain, log_gamma
    )
    partial_rows = jnp.dot(
        retained,
        lax.all_gather(w_out, "ep", axis=1, tiled=True),
        preferred_element_type=jnp.float32,
    )
    rounded = lax.optimization_barrier(partial_rows.astype(jnp.bfloat16)).astype(jnp.float32)
    mixer_out = (
        over_copies(rounded.astype(jnp.bfloat16), "tp").astype(jnp.float32).astype(jnp.bfloat16)
    )
    residual_sum = (inputs.astype(jnp.float32) + mixer_out.astype(jnp.float32)).astype(jnp.bfloat16)
    normed_ffn = rms_scale(residual_sum, norm_ffn)
    slot_index = slot_of(route_ids, expert_count, capacity)
    slot_total = expert_count * capacity
    placing = (jnp.arange(slot_total, dtype=jnp.int32)[:, None] == slot_index[None, :]).astype(
        jnp.float32
    )
    by_token = jnp.sum(placing.reshape(slot_total, seq_count, top_count), axis=2)
    outgoing = (
        jnp.dot(by_token.astype(jnp.bfloat16), normed_ffn, preferred_element_type=jnp.float32)
        .astype(jnp.bfloat16)
        .reshape(expert_count, capacity, D)
    )
    received = lax.all_to_all(outgoing, "ep", split_axis=0, concat_axis=0, tiled=True)
    slot_count = received.shape[1]
    grouped = received.reshape(ep_size, local_experts, slot_count, D)
    gate_part = jnp.einsum("sjnd,jdf->sjnf", grouped, exp_gate, preferred_element_type=jnp.float32)
    up_part = jnp.einsum("sjnd,jdf->sjnf", grouped, exp_up, preferred_element_type=jnp.float32)
    hidden = (jax.nn.silu(gate_part) * up_part).astype(jnp.bfloat16)
    partial_out = jnp.einsum(
        "sjnf,jfd->sjnd", hidden, exp_down, preferred_element_type=jnp.float32
    ).reshape(received.shape[0], slot_count, D)
    returned = lax.all_to_all(
        partial_out.astype(jnp.bfloat16), "ep", split_axis=0, concat_axis=0, tiled=True
    ).astype(partial_out.dtype)
    widened = route_weight.astype(jnp.float32)
    share_flat = (widened / jnp.sum(widened, axis=-1, keepdims=True)).reshape(-1)
    weighting = jnp.sum(
        (placing * share_flat[None, :]).reshape(slot_total, seq_count, top_count), axis=2
    )
    expert_part = jnp.einsum(
        "rt,rd->td", weighting, returned.reshape(slot_total, D), precision=lax.Precision.HIGHEST
    )
    segment = lax.all_gather(normed_ffn, "ep", axis=0, tiled=True)
    gate_part = jnp.dot(segment, dense_gate, preferred_element_type=jnp.float32)
    up_part = jnp.dot(segment, dense_up, preferred_element_type=jnp.float32)
    hidden = (jax.nn.silu(gate_part) * up_part).astype(jnp.bfloat16)
    opening = jax.nn.sigmoid(
        jnp.dot(segment, branch_gate[:, None], preferred_element_type=jnp.float32)
    )
    branch_term = jnp.dot(hidden, dense_down, preferred_element_type=jnp.float32) * opening
    summed_branch = summed_on_arrival(branch_term.astype(jnp.bfloat16), "ep", 0)
    summed_branch = summed_branch + expert_part
    width_total = over_copies(summed_branch.astype(jnp.bfloat16), "tp").astype(jnp.float32)
    layer_out = (residual_sum.astype(jnp.float32) + width_total).astype(jnp.bfloat16)
    return (layer_out, new_state)


def solution(mesh):
    in_specs = (
        P("ep", None),
        P("ep"),
        P("ep", "tp", None, None),
        P(),
        P("ep", "tp"),
        P("ep", "tp"),
        P("ep", "tp"),
        P("ep", "tp"),
        P("tp"),
        P("tp", "ep"),
        P(),
        P("ep", None),
        P("ep", None),
        P("ep", None, "tp"),
        P("ep", None, "tp"),
        P("ep", "tp", None),
        P(None, ("ep", "tp")),
        P(None, ("ep", "tp")),
        P(("ep", "tp"), None),
        P(),
    )
    out_specs = (P("ep", None), P("ep", "tp", None, None))
    return jax.shard_map(
        on_device, mesh=mesh, in_specs=in_specs, out_specs=out_specs, check_vma=False
    )
```

profile of v0, /device:TPU:1, one launch (start us, length us, event | category | flops | bytes accessed | tf_op | source)
XLA Modules:
  0.0 340.6 jit_solution(12423903585357650774)
XLA Ops:
  7.2 1.7 pad_maximum_fusion
  9.0 0.7 all-gather.6.cloned.1.call-update
  9.8 0.7 convert_element_type.100
  10.5 0.7 convert_element_type.103
  11.1 0.7 convert_element_type.113
  11.9 1.0 fusion.64
  12.9 0.7 bitcast_convert_fusion
  13.6 0.1 multiply_cosine_fusion
  13.7 91.6 %all-gather.4.cloned.1.call-done = bf16[2048,3072]{1,0:T(8,128)(2,1)} async-done(((bf16[32,3072]{1,0:T(8,128)(2,1)}), bf16[2048,3072]{1,0:T(8,128)(2,1)}) %all-gather.4.cloned.1.call-update) | async-done | bytes 12582928 | tf_op jit(solution)/shard_map/all_gather | solution.py:15
  105.3 2.5 fusion.33
  107.8 2.5 fusion.39
  110.4 2.4 fusion.45
  112.8 0.1 multiply_subtract_fusion.1
  112.9 0.1 maximum_multiply_fusion
  113.1 4.5 %multiply_add_fusion = f32[16,6,128,128]{3,2,1,0:T(8,128)S(1)} fusion(f32[16,6,128,128]{3,2,1,0:T(8,128)} %param.22, f32[16,6,128]{2,1,0:T(8,128)S(1)} %reshape.207, f32[16,6,128]{2,1,0:T(8,128)S(1)} %maximum_multiply_fusion, f32[6]{0:T(128)S(1)} %dynamic-slice_exponential_fusion), kind=kLoop, calls=%fused_computation.2 | loop fusion | flops 4718592 | bytes 12681240 | tf_op jit(solution)/shard_map/add | solution.py:82
  117.6 2.7 copy-done.2
  120.3 5.5 %fusion.84 = f32[16,6,1,128]{3,2,1,0:T(1,128)S(1)} fusion(f32[16,6,128,128]{3,2,1,0:T(8,128)S(1)} %multiply_add_fusion, f32[16,6,128,1]{2,1,0,3:T(8,128)S(1)} %maximum_bitcast_fusion), kind=kOutput, calls=%fused_computation.80 | convolution fusion | flops 18874368 | bytes 6389760 | tf_op jit(solution)/shard_map/shd,shdv->shv/dot_general | solution.py:85
  125.8 0.1 bitcast_reduce_fusion
  125.9 0.2 fusion.80
  126.0 0.1 fusion.81
  126.2 47.2 %all-gather.6.cloned.1.call-done = bf16[768,2048]{0,1:T(8,128)(2,1)} async-done(((bf16[768,32]{0,1:T(8,128)(2,1)}), bf16[768,2048]{0,1:T(8,128)(2,1)}) %all-gather.6.cloned.1.call-update) | async-done | bytes 3145744 | tf_op jit(solution)/shard_map/all_gather | solution.py:150
  173.4 4.5 %convolution_convert_fusion.2 = bf16[16,2048]{1,0:T(8,128)(2,1)S(1)} fusion(bf16[768,2048]{0,1:T(8,128)(2,1)} %all-gather.6.cloned.1.call-done, f32[2,8,6,128]{3,2,1,0:T(8,128)S(1)} %bitcast.87, bf16[2048,3072]{1,0:T(8,128)(2,1)} %all-gather.4.cloned.1.call-done, bf16[16,2048]{1,0:T(8,128)(2,1)S(1)} %copy-done.3, f32[2048]{0:T(1024)S(1)} %convert_element_type.100, ...), kind=kOutput, calls=%fused_computation.15 | convolution fusion | flops 100925440 | bytes 6479936 | tf_op jit(solution)/shard_map/dot_general | solution.py:148
  177.9 5.7 %all_to_all.25 = bf16[2,16,2048]{2,1,0:T(8,128)(2,1)S(1)} all-to-all(bf16[2,16,2048]{2,1,0:T(8,128)(2,1)S(1)} %broadcast_in_dim.4), channel_id=1, replica_groups=mesh['ep'=64,'tp'=2] {'tp'}, dimensions={0} | all-to-all | bytes 262144 | tf_op jit(solution)/shard_map/all_to_all | solution.py:24
  183.6 0.1 fusion.68
  183.8 0.7 fusion.70
  184.6 0.1 eq.31
  184.8 0.1 reduce_window_sum.11
  184.9 0.2 select_reduce_fusion.1
  185.1 0.1 copy.44
  185.4 1.2 convolution_convert_fusion.1
  186.5 1.1 reshape.197
  187.7 6.1 %all-to-all-start.2 = ((bf16[64,2,2048]{2,1,0:T(2,128)(2,1)}), bf16[64,2,2048]{2,1,0:T(2,128)(2,1)S(1)}, u32[]{:S(2)}, u32[]{:S(2)}) async-start(bf16[64,2,2048]{2,1,0:T(2,128)(2,1)} %reshape.197), calls=%async_computation.2 | async-start | bytes 1048576 | tf_op jit(solution)/shard_map/all_to_all | solution.py:170
  193.8 12.9 %all-to-all-done.2 = bf16[64,2,2048]{2,1,0:T(2,128)(2,1)S(1)} async-done(((bf16[64,2,2048]{2,1,0:T(2,128)(2,1)}), bf16[64,2,2048]{2,1,0:T(2,128)(2,1)S(1)}, u32[]{:S(2)}, u32[]{:S(2)}) %all-to-all-start.2) | async-done | bytes 524320 | tf_op jit(solution)/shard_map/all_to_all | solution.py:170
  206.7 2.0 fusion.14
  208.8 2.4 convolution_convert_fusion
  211.2 1.4 copy.47
  212.6 4.8 %all-to-all-start.3 = ((bf16[64,2,2048]{2,1,0:T(2,128)(2,1)}), bf16[64,2,2048]{2,1,0:T(2,128)(2,1)S(1)}, u32[]{:S(2)}, u32[]{:S(2)}) async-start(bf16[64,2,2048]{2,1,0:T(2,128)(2,1)} %copy.47), calls=%async_computation.3 | async-start | bytes 1048576 | tf_op jit(solution)/shard_map/all_to_all | solution.py:179
  217.5 36.3 %all-gather.8.cloned.1.call-done = bf16[1024,2048]{1,0:T(8,128)(2,1)} async-done(((bf16[16,2048]{1,0:T(8,128)(2,1)}), bf16[1024,2048]{1,0:T(8,128)(2,1)}) %all-gather.8.cloned.1.call-update) | async-done | bytes 4194320 | tf_op jit(solution)/shard_map/all_gather | solution.py:190
  253.8 3.7 %fusion.101 = f32[1024,32]{0,1:T(8,128)S(1)} fusion(bf16[1024,2048]{1,0:T(8,128)(2,1)} %all-gather.8.cloned.1.call-done, bf16[2048,32]{0,1:T(8,128)(2,1)} %param.36), kind=kOutput, calls=%fused_computation.107 | convolution fusion | flops 134217728 | bytes 4456448 | tf_op jit(solution)/shard_map/dot_general | solution.py:191
  257.5 1.2 fusion.102
  258.7 6.7 %multiply_convert_fusion = bf16[1024,2048]{1,0:T(8,128)(2,1)} fusion(bf16[32,2048]{1,0:T(8,128)(2,1)S(1)} %copy-done.4, f32[1024]{0:T(1024)S(1)} %add_divide_fusion, bf16[1024,2048]{1,0:T(8,128)(2,1)} %all-gather.8.cloned.1.call-done, bf16[2048,32]{0,1:T(8,128)(2,1)S(1)} %copy-done.5, f32[1024,32]{0,1:T(8,128)S(1)} %fusion.101), kind=kOutput, calls=%fused_computation.1 | convolution fusion | flops 272826368 | bytes 8785920 | tf_op jit(solution)/shard_map/dot_general | solution.py:197
  265.4 6.8 %all-to-all-start.1 = ((bf16[64,16,2048]{2,1,0:T(8,128)(2,1)}), bf16[64,16,2048]{2,1,0:T(8,128)(2,1)}, u32[]{:S(2)}, u32[]{:S(2)}) async-start(bf16[64,16,2048]{2,1,0:T(8,128)(2,1)} %bitcast.86), calls=%async_computation.1 | async-start | bytes 8388608 | tf_op jit(solution)/shard_map/all_to_all | solution.py:39
  272.2 0.2 reshape.202
  272.4 50.4 %all-to-all-done.1 = bf16[64,16,2048]{2,1,0:T(8,128)(2,1)} async-done(((bf16[64,16,2048]{2,1,0:T(8,128)(2,1)}), bf16[64,16,2048]{2,1,0:T(8,128)(2,1)}, u32[]{:S(2)}, u32[]{:S(2)}) %all-to-all-start.1) | async-done | bytes 4194336 | tf_op jit(solution)/shard_map/all_to_all | solution.py:39
  322.8 2.9 convert_reduce_fusion
  325.6 0.3 fusion.8
  326.0 7.5 %all_to_all.26 = bf16[2,16,2048]{2,1,0:T(8,128)(2,1)S(1)} all-to-all(bf16[2,16,2048]{2,1,0:T(8,128)(2,1)S(1)} %broadcast_in_dim.5), channel_id=1, replica_groups=mesh['ep'=64,'tp'=2] {'tp'}, dimensions={0} | all-to-all | bytes 262144 | tf_op jit(solution)/shard_map/all_to_all | solution.py:24
  333.4 0.7 fusion.71
  (47 shorter events, 0.9 us)
Async XLA Ops:
  7.2 201.6 %copy-start = (bf16[1,512,2048]{2,1,0:T(8,128)(2,1)S(1)}, bf16[1,512,2048]{2,1,0:T(8,128)(2,1)}, u32[]{:S(2)}) copy-start(bf16[1,512,2048]{2,1,0:T(8,128)(2,1)} %param.35) | copy-start | bytes 6291460
  7.2 103.2 %copy-start.3 = (bf16[16,2048]{1,0:T(8,128)(2,1)S(1)}, bf16[16,2048]{1,0:T(8,128)(2,1)}, u32[]{:S(2)}) copy-start(bf16[16,2048]{1,0:T(8,128)(2,1)} %param.20) | copy-start | bytes 196612
  7.2 98.1 %all-gather.4.cloned.1.call-start = ((), (), s32[]{:S(2)}) async-start(), calls=%async_computation.5 | async-start | bytes 12779520 | tf_op jit(solution)/shard_map/all_gather | solution.py:15
  9.0 164.4 %all-gather.6.cloned.1.call-start = ((), (), s32[]{:S(2)}) async-start(), calls=%async_computation.6 | async-start | bytes 3194880 | tf_op jit(solution)/shard_map/all_gather | solution.py:150
  9.7 244.0 %all-gather.8.cloned.1.call-start = ((), (), s32[]{:S(2)}) async-start(), calls=%async_computation.7 | async-start | bytes 4259840 | tf_op jit(solution)/shard_map/all_gather | solution.py:190
  117.6 2.7 copy-start.2
  125.7 58.8 %copy-start.6 = (s32[16,4]{0,1:T(4,128)S(1)}, s32[16,4]{0,1:T(4,128)}, u32[]{:S(2)}) copy-start(s32[16,4]{0,1:T(4,128)} %param.31) | copy-start | bytes 772
  125.8 59.5 %copy-start.8 = (bf16[16,4]{0,1:T(4,128)(2,1)S(1)}, bf16[16,4]{0,1:T(4,128)(2,1)}, u32[]{:S(2)}) copy-start(bf16[16,4]{0,1:T(4,128)(2,1)} %param.32) | copy-start | bytes 388
  173.4 20.4 %copy-start.7 = (bf16[2048]{0:T(1024)(128)(2,1)S(1)}, bf16[2048]{0:T(1024)(128)(2,1)}, u32[]{:S(2)}) copy-start(bf16[2048]{0:T(1024)(128)(2,1)} %param.39) | copy-start | bytes 12292
  187.7 19.0 %all-to-all-start.2 = ((bf16[64,2,2048]{2,1,0:T(2,128)(2,1)}), bf16[64,2,2048]{2,1,0:T(2,128)(2,1)S(1)}, u32[]{:S(2)}, u32[]{:S(2)}) async-start(bf16[64,2,2048]{2,1,0:T(2,128)(2,1)} %reshape.197), calls=%async_computation.2 | async-start | bytes 1048576 | tf_op jit(solution)/shard_map/all_to_all | solution.py:170
  212.6 52.8 %all-to-all-start.3 = ((bf16[64,2,2048]{2,1,0:T(2,128)(2,1)}), bf16[64,2,2048]{2,1,0:T(2,128)(2,1)S(1)}, u32[]{:S(2)}, u32[]{:S(2)}) async-start(bf16[64,2,2048]{2,1,0:T(2,128)(2,1)} %copy.47), calls=%async_computation.3 | async-start | bytes 1048576 | tf_op jit(solution)/shard_map/all_to_all | solution.py:179
  217.4 41.2 %copy-start.4 = (bf16[32,2048]{1,0:T(8,128)(2,1)S(1)}, bf16[32,2048]{1,0:T(8,128)(2,1)}, u32[]{:S(2)}) copy-start(bf16[32,2048]{1,0:T(8,128)(2,1)} %param.38) | copy-start | bytes 393220
  217.4 41.2 %copy-start.5 = (bf16[2048,32]{0,1:T(8,128)(2,1)S(1)}, bf16[2048,32]{0,1:T(8,128)(2,1)}, u32[]{:S(2)}) copy-start(bf16[2048,32]{0,1:T(8,128)(2,1)} %param.37) | copy-start | bytes 393220
  253.8 3.7 %copy-start.1 = (bf16[1024,2048]{1,0:T(8,128)(2,1)S(1)}, bf16[1024,2048]{1,0:T(8,128)(2,1)}, u32[]{:S(2)}) copy-start(bf16[1024,2048]{1,0:T(8,128)(2,1)} %all-gather.8.cloned.1.call-done) | copy-start | bytes 12582916
  265.4 57.4 %all-to-all-start.1 = ((bf16[64,16,2048]{2,1,0:T(8,128)(2,1)}), bf16[64,16,2048]{2,1,0:T(8,128)(2,1)}, u32[]{:S(2)}, u32[]{:S(2)}) async-start(bf16[64,16,2048]{2,1,0:T(8,128)(2,1)} %bitcast.86), calls=%async_computation.1 | async-start | bytes 8388608 | tf_op jit(solution)/shard_map/all_to_all | solution.py:39
Sparse Core Ops, SparseCore 0:
  11.3 93.9 all-gather.3
  108.1 65.2 all-gather.5
  184.6 69.0 all-gather.7
where the time goes:
time: 341 us
  waiting for transfers between devices  239 us (70%)
  matrix products  34.9 us (10%)
  starting transfers between devices  17.9 us (5%)
  other arithmetic  15.6 us (5%)
  between operations  14.1 us (4%)
  blocking collectives  13.2 us (4%)
  local copies, waits for them, and re-layouts  6 us (2%)
    all_gather x1, waiting for transfers between devices, in_one_piece(): out, at, done = (lax.all_gather(both, axis, axis=dim, tiled=True), 0, [])  91.6 us
    all_to_all x1, waiting for transfers between devices, summed_on_arrival(): tiles = lax.all_to_all(split_up(array, dim, size), axis, 0, 0, tiled=True)  50.4 us
    all_gather x1, waiting for transfers between devices, on_device(): lax.all_gather(w_out, 'ep', axis=1, tiled=True)  47.2 us
    all_gather x1, waiting for transfers between devices, on_device(): segment = lax.all_gather(normed_ffn, 'ep', axis=0, tiled=True)  36.3 us
    all_to_all x2, blocking collectives, sent_to_all(): return lax.all_to_all(copies, axis, split_axis=0, concat_axis=0, tiled=True)  13.2 us
    all_to_all x1, waiting for transfers between devices, on_device(): lax.all_to_all(outgoing, 'ep', split_axis=0, concat_axis=0, tiled=True)  12.9 us
    dot_general x3, matrix products, on_device(): jnp.dot(normed, weight_rows, preferred_element_type=jnp.float32)  7.44 us
  transfers between devices with their start and end apart: 6, of which 5 were waited for; matrix products, arithmetic and copies ran while one was open for 13% of the time, Pallas kernels for 0%

commit v1 on v0

v1 whole, which is shorter than its diff:
```python
import functools

import jax
import jax.numpy as jnp
from jax import lax
from jax.experimental import pallas as pl
from jax.experimental.pallas import tpu as pltpu
from jax.sharding import PartitionSpec as P

D = 2048
HEADS = 12
HD = 128
LH = 6
RW = 768
T = 16
NZ = 4
NP = 16
EPS = 1e-06
MESH = pl.DeviceIdType.MESH
F32 = jnp.float32
BF16 = jnp.bfloat16
NT = (((1,), (1,)), ((), ()))
ANY = pl.BlockSpec(memory_space=pl.ANY)
VM = pl.BlockSpec(memory_space=pltpu.VMEM)
SM = pl.BlockSpec(memory_space=pltpu.SMEM)


class Links:
    def __init__(self, send, recv, local):
        ep = lax.axis_index("ep")
        self.c = lax.axis_index("tp")
        self.z = ep // NP
        self.p = ep % NP
        self.y = self.p // 4
        self.x = self.p % 4
        self.send, self.recv, self.local = send, recv, local
        self.n = 0
        self.m = 0

    def plane(self, d):
        return ((self.y + d // 4) % 4) * 4 + (self.x + d % 4) % 4

    def chip(self, z, p):
        return z * NP + p

    def push(self, src, dst, ep, tp):
        k = self.n
        self.n += 1
        copy = pltpu.make_async_remote_copy(
            src_ref=src,
            dst_ref=dst,
            send_sem=self.send.at[k],
            recv_sem=self.recv.at[k],
            device_id=(ep, tp),
            device_id_type=MESH,
        )
        copy.start()
        return copy

    def pull(self, src, dst):
        k = self.m
        self.m += 1
        copy = pltpu.make_async_copy(src, dst, self.local.at[k])
        copy.start()
        return copy

    def barrier_signal(self, both_cores):
        bar = pltpu.get_barrier_semaphore()
        peers = [(self.chip(self.z, self.plane(d)), self.c) for d in range(1, NP)]
        peers += [(self.chip((self.z + k) % NZ, self.p), self.c) for k in range(1, NZ)]
        if both_cores:
            peers += [(self.chip((self.z + k) % NZ, self.p), 1 - self.c) for k in range(NZ)]
        for peer in peers:
            pl.semaphore_signal(bar, inc=1, device_id=peer, device_id_type=MESH)
        return bar, len(peers)


def rms(values, scales):
    scaled = values * lax.rsqrt(jnp.mean(values * values, axis=-1, keepdims=True) + EPS)
    return (scaled * scales.astype(F32)).astype(BF16)


def project_kernel(
    x_ref, gain_ref, wq, wk, wv, wg, wo_in, dg_in, du_in, dd_in,
    q_ref, wo_out, dw_out,
    xs, xg, wz, wo_own, d_own, part, rsl, send, recv, local,
):
    at = Links(send, recv, local)
    z, p, c = at.z, at.p, at.c
    bar, greeted = at.barrier_signal(False)
    w_copies = [
        at.pull(w, wz.at[z, :, j * RW : (j + 1) * RW]) for j, w in enumerate((wq, wk, wv, wg))
    ]
    wo_copy = at.pull(wo_in, wo_own)
    d_copies = [at.pull(w, d_own.at[j]) for j, w in enumerate((dg_in, du_in, dd_in))]
    n = rms(x_ref[...].astype(F32), gain_ref[...]).astype(F32)
    lane_block = lax.broadcasted_iota(jnp.int32, (T, 128), 1) // 32
    for y in range(4):
        for x in range(4):
            piece = jnp.zeros((T, 128), F32)
            for k in range(NZ):
                tile = n[:, k * 512 + y * 128 : k * 512 + (y + 1) * 128]
                turn = ((k - x) * 32) % 128
                if turn:
                    tile = pltpu.roll(tile, turn, 1)
                piece = jnp.where(lane_block == k, tile, piece)
            xs[y * 4 + x] = piece.astype(BF16)
    xg[0] = xs[p]
    pl.semaphore_wait(bar, greeted)
    up, down = (z + 1) % NZ, (z + 3) % NZ
    for copy in w_copies:
        copy.wait()
    w_up = at.push(wz.at[z], wz.at[z], at.chip(up, p), c)
    w_down = at.push(wz.at[z], wz.at[z], at.chip(down, p), c)
    x_sends = []
    for d in range(1, NP):
        q = at.plane(d)
        x_sends.append(at.push(xs.at[q], xg.at[d], at.chip(z, q), c))
    wo_copy.wait()
    wo_keep = at.pull(wo_own, wo_out.at[p])
    wo_sends = []
    for d in range(1, NP):
        q = at.plane(d)
        wo_sends.append(at.push(wo_own, wo_out.at[p], at.chip(z, q), c))
    half = 2 * RW
    w_up.wait_recv()
    w_up2 = at.push(wz.at[down, :, :half], wz.at[down, :, :half], at.chip(up, p), c)
    w_down.wait_recv()
    w_down2 = at.push(wz.at[up, :, half:], wz.at[up, :, half:], at.chip(down, p), c)
    for copy in d_copies:
        copy.wait()
    d_keep = at.pull(d_own, dw_out.at[z])
    d_up = at.push(d_own, dw_out.at[z], at.chip(up, p), c)
    d_down = at.push(d_own, dw_out.at[z], at.chip(down, p), c)
    for copy in x_sends:
        copy.wait_recv()
    w_up2.wait_recv()
    w_down2.wait_recv()
    rows = xg[...].reshape(NP * T, 128)
    for j in range(4):
        cols = slice(j * RW, (j + 1) * RW)
        w = wz[:, :, cols].reshape(128, RW)
        prod = jnp.dot(rows, w, preferred_element_type=F32)
        part[:, :, cols] = prod.astype(BF16).reshape(NP, T, RW)
    r_sends = []
    for d in range(1, NP):
        back = (((at.y + 4 - d // 4) % 4) * 4) + (at.x + 4 - d % 4) % 4
        r_sends.append(at.push(part.at[d], rsl.at[d], at.chip(z, back), c))
    d_up.wait_recv()
    d_up2 = at.push(
        dw_out.at[down, :, :, :1024], dw_out.at[down, :, :, :1024], at.chip(up, p), c
    )
    d_down.wait_recv()
    d_down2 = at.push(dw_out.at[up, :, :, 1024:], dw_out.at[up, :, :, 1024:], at.chip(down, p), c)
    total = part[0].astype(F32)
    for d in range(1, NP):
        r_sends[d - 1].wait_recv()
        total = total + rsl[d].astype(F32)
    q_ref[...] = total.astype(BF16)
    for copy in wo_sends + [d_up2, d_down2]:
        copy.wait_recv()
    for copy in [w_up, w_down, w_up2, w_down2, d_up, d_down, d_up2, d_down2]:
        copy.wait_send()
    for copy in x_sends + wo_sends + r_sends:
        copy.wait_send()
    wo_keep.wait()
    d_keep.wait()


def project(x, gain, wq, wk, wv, wg, wo_t, dg_t, du_t, dd):
    return pl.pallas_call(
        project_kernel,
        out_shape=(
            jax.ShapeDtypeStruct((T, 4 * RW), BF16),
            jax.ShapeDtypeStruct((NP, 32, RW), BF16),
            jax.ShapeDtypeStruct((NZ, 3, 32, D), BF16),
        ),
        in_specs=[VM, VM] + [ANY] * 8,
        out_specs=(VM, ANY, ANY),
        scratch_shapes=[
            pltpu.VMEM((NP, T, 128), BF16),
            pltpu.VMEM((NP, T, 128), BF16),
            pltpu.VMEM((NZ, 32, 4 * RW), BF16),
            pltpu.VMEM((32, RW), BF16),
            pltpu.VMEM((3, 32, D), BF16),
            pltpu.VMEM((NP, T, 4 * RW), BF16),
            pltpu.VMEM((NP, T, 4 * RW), BF16),
            pltpu.SemaphoreType.DMA((56,)),
            pltpu.SemaphoreType.DMA((56,)),
            pltpu.SemaphoreType.DMA((12,)),
        ],
        compiler_params=pltpu.CompilerParams(collective_id=0, has_side_effects=True),
        name="project",
    )(x, gain, wq, wk, wv, wg, wo_t, dg_t, du_t, dd)


STEP = 2


def state_kernel(q_ref, cos_ref, sin_ref, gain_ref, gamma_ref, s_ref, ret_ref, new_ref, qk, vv, ro):
    i = pl.program_id(0)

    @pl.when(i == 0)
    def _():
        cosine, sine = cos_ref[...], sin_ref[...]
        for h in range(LH):
            for part, row, scale in ((0, 0, None), (1, 8, HD**-0.5)):
                f = q_ref[:, part * RW + h * HD : part * RW + (h + 1) * HD].astype(F32)
                turned = f * cosine + pltpu.roll(f, 64, 1) * sine
                if scale is not None:
                    turned = turned * scale
                qk[:, row + h, :] = turned
            vv[:, h, :] = q_ref[:, 2 * RW + h * HD : 2 * RW + (h + 1) * HD].astype(F32)

    for t in range(STEP):
        tok = i * STEP + t
        columns = qk[tok].T
        v = vv[tok]
        for h in range(LH):
            new = gamma_ref[h] * s_ref[t, h] + columns[:, 8 + h : 9 + h] * v[h : h + 1, :]
            new_ref[t, h] = new
            ro[tok, h : h + 1, :] = jnp.sum(columns[:, h : h + 1] * new, axis=0, keepdims=True)

    @pl.when(i == pl.num_programs(0) - 1)
    def _():
        for h in range(LH):
            cols = slice(h * HD, (h + 1) * HD)
            r = ro[:, h, :]
            centred = r - jnp.mean(r, axis=-1, keepdims=True)
            normed = centred * lax.rsqrt(jnp.mean(centred * centred, axis=-1, keepdims=True) + EPS)
            normed = normed * gain_ref[:, cols].astype(F32)
            gate = q_ref[:, 3 * RW + h * HD : 3 * RW + (h + 1) * HD].astype(F32)
            ret_ref[:, cols] = (normed * (gate * jax.nn.sigmoid(gate))).astype(BF16)


def update(qkvg, cosine, sine, gain, gamma, state):
    whole = lambda shape: pl.BlockSpec(shape, lambda i: (0,) * len(shape))
    block = pl.BlockSpec((STEP, LH, HD, HD), lambda i: (i, 0, 0, 0))
    return pl.pallas_call(
        state_kernel,
        grid=(T // STEP,),
        out_shape=(
            jax.ShapeDtypeStruct((T, RW), BF16),
            jax.ShapeDtypeStruct((T, LH, HD, HD), F32),
        ),
        in_specs=[
            whole((T, 4 * RW)), whole((T, HD)), whole((T, HD)), whole((1, RW)), SM, block,
        ],
        out_specs=(whole((T, RW)), block),
        scratch_shapes=[
            pltpu.VMEM((T, 16, HD), F32),
            pltpu.VMEM((T, 8, HD), F32),
            pltpu.VMEM((T, 8, HD), F32),
        ],
        name="state",
    )(qkvg, cosine, sine, gain, gamma, state)


def silu(x):
    return x * jax.nn.sigmoid(x)


def ffn_kernel(
    ret_ref, x_ref, gain_ref, bg_ref, sel_ref, wo_in, dw_in, eg_in, eu_in, ed_in,
    out_ref,
    wo, dgt, dut, ddn, eg, eu, ed,
    retz, mo, mx, nf, xp, selg, seb, ein, eo, eop, er, rin, dp, dpp, po, rsl, lo,
    send, recv, local,
):
    at = Links(send, recv, local)
    z, p, c = at.z, at.p, at.c
    o = 1 - c
    me = at.chip(z, p)
    bar, greeted = at.barrier_signal(True)
    wo_copy = at.pull(wo_in, wo)
    e_copies = [at.pull(a, b) for a, b in ((eg_in, eg), (eu_in, eu), (ed_in, ed))]
    d_copies = [at.pull(dw_in.at[:, j], w) for j, w in enumerate((dgt, dut, ddn))]
    retz[z] = ret_ref[...]
    selg[0] = sel_ref[0]
    pl.semaphore_wait(bar, greeted)
    sends = []

    def push(*args):
        copy = at.push(*args)
        sends.append(copy)
        return copy

    ret_copies = [push(ret_ref, retz.at[z], at.chip((z + k) % NZ, p), c) for k in range(1, NZ)]
    sel_copies = [push(sel_ref.at[d], selg.at[d], at.chip(z, at.plane(d)), c) for d in range(1, NP)]
    wo_copy.wait()
    for copy in ret_copies:
        copy.wait_recv()
    mixed = lax.dot_general(
        retz[...].reshape(NZ * T, RW), wo[...].reshape(512, RW), NT, preferred_element_type=F32
    )
    mo[...] = mixed.astype(BF16).reshape(NZ, T, 512)
    mx[c, z] = mo[z]
    mx_copies = [push(mo.at[z], mx.at[c, z], me, o)]
    for k in range(1, NZ):
        to = (z + k) % NZ
        for core in (c, o):
            mx_copies.append(push(mo.at[to], mx.at[c, z], at.chip(to, p), core))
    for copy in mx_copies:
        copy.wait_recv()
    mixer = [(mx[0, k].astype(F32) + mx[1, k].astype(F32)).astype(BF16) for k in range(NZ)]
    mixer_out = jnp.concatenate(mixer, axis=-1).astype(F32)
    residual = (x_ref[...].astype(F32) + mixer_out).astype(BF16)
    normed = rms(residual.astype(F32), gain_ref[...])
    for h in range(2):
        nf[h] = normed[:, h * 1024 : (h + 1) * 1024]
        xp[h, 0] = normed[:, h * 1024 : (h + 1) * 1024]
        lo[h] = residual[:, h * 1024 : (h + 1) * 1024]

    x_copies = [
        push(nf.at[c], xp.at[c, d], at.chip(z, at.plane(d)), c) for d in range(1, NP)
    ]
    for copy in sel_copies:
        copy.wait_recv()
    weights = selg[...].reshape(NP * T, 128)
    w_hi = weights.astype(BF16)
    w_lo = (weights - w_hi.astype(F32)).astype(BF16)
    chosen = jnp.where(weights.T > 0.0, 1.0, 0.0).astype(BF16)
    f_copies = []
    for d in range(1, NP):
        x_copies[d - 1].wait_recv()
        f_copies.append(push(xp.at[c, d], xp.at[c, d], me, o))
    picked = jnp.dot(chosen, xp[c].reshape(NP * T, 1024), preferred_element_type=F32)
    seb[...] = picked.astype(BF16).reshape(NZ, 32, 1024)
    ein[c, z] = seb[z]
    e_out = [
        push(seb.at[(z + k) % NZ], ein.at[c, z], at.chip((z + k) % NZ, p), c) for k in range(1, NZ)
    ]
    e_pair = [push(seb.at[z], ein.at[c, z], me, o)]

    for copy in d_copies:
        copy.wait()
    for copy in f_copies:
        copy.wait_recv()
    gate = jnp.zeros((NP * T, 128), F32)
    up = jnp.zeros((NP * T, 128), F32)
    opening = jnp.zeros((NP * T, 1), F32)
    for h in range(2):
        cols = slice(h * 1024, (h + 1) * 1024)
        block = xp[h].reshape(NP * T, 1024)
        gate = gate + lax.dot_general(
            block, dgt[:, :, cols].reshape(128, 1024), NT, preferred_element_type=F32
        )
        up = up + lax.dot_general(
            block, dut[:, :, cols].reshape(128, 1024), NT, preferred_element_type=F32
        )
        opening = opening + jnp.sum(
            block.astype(F32) * bg_ref[:, cols].astype(F32), axis=-1, keepdims=True
        )
    opening = jax.nn.sigmoid(opening)
    hidden = (silu(gate) * up).astype(BF16)
    down = ddn[...].reshape(128, D)
    for h in range(2):
        term = jnp.dot(
            hidden, down[:, h * 1024 : (h + 1) * 1024], preferred_element_type=F32
        )
        dp[h] = (term * opening).astype(BF16)
    dp_copy = push(dp.at[o], dpp, me, o)

    for k in range(1, NZ):
        e_out[k - 1].wait_recv()
        frm = (z + NZ - k) % NZ
        e_pair.append(push(ein.at[c, frm], ein.at[c, frm], me, o))
    for copy in e_copies:
        copy.wait()
    for copy in e_pair:
        copy.wait_recv()
    gate = jnp.zeros((128, 512), F32)
    up = jnp.zeros((128, 512), F32)
    for h in range(2):
        block = ein[h].reshape(128, 1024)
        rows = slice(h * 1024, (h + 1) * 1024)
        gate = gate + jnp.dot(block, eg[rows, :], preferred_element_type=F32)
        up = up + jnp.dot(block, eu[rows, :], preferred_element_type=F32)
    hidden = (silu(gate) * up).astype(BF16)
    for h in range(2):
        eo[h] = jnp.dot(
            hidden, ed[:, h * 1024 : (h + 1) * 1024], preferred_element_type=F32
        ).astype(BF16)
    eo_copy = push(eo.at[o], eop, me, o)
    eo_copy.wait_recv()
    er[...] = (eo[c].astype(F32) + eop[...].astype(F32)).astype(BF16).reshape(NZ, 32, 1024)
    rin[z] = er[z]
    r_copies = [
        push(er.at[(z + k) % NZ], rin.at[z], at.chip((z + k) % NZ, p), c) for k in range(1, NZ)
    ]
    dp_copy.wait_recv()
    for copy in r_copies:
        copy.wait_recv()
    results = rin[...].reshape(128, 1024)
    total = jnp.dot(w_hi, results, preferred_element_type=F32)
    total = total + jnp.dot(w_lo, results, preferred_element_type=F32)
    total = total + (dp[c].astype(F32) + dpp[...].astype(F32))
    po[...] = total.astype(BF16).reshape(NP, T, 1024)
    s_copies = []
    for d in range(1, NP):
        back = (((at.y + 4 - d // 4) % 4) * 4) + (at.x + 4 - d % 4) % 4
        s_copies.append(push(po.at[d], rsl.at[d], at.chip(z, back), c))
    total = po[0].astype(F32)
    for d in range(1, NP):
        s_copies[d - 1].wait_recv()
        total = total + rsl[d].astype(F32)
    nf_out = (lo[c].astype(F32) + total).astype(BF16)
    lo[2] = nf_out
    l_copy = push(lo.at[2], lo.at[3], me, o)
    l_copy.wait_recv()
    mine, other = nf_out, lo[3]
    first = jnp.where(c == 0, mine, other)
    second = jnp.where(c == 0, other, mine)
    out_ref[:, :1024] = first
    out_ref[:, 1024:] = second
    for copy in sends:
        copy.wait_send()


def ffn(ret, x, gain, bg, sel, wo, dw, eg, eu, ed):
    v = lambda shape, dtype=BF16: pltpu.VMEM(shape, dtype)
    return pl.pallas_call(
        ffn_kernel,
        out_shape=jax.ShapeDtypeStruct((T, D), BF16),
        in_specs=[VM] * 5 + [ANY] * 5,
        out_specs=VM,
        scratch_shapes=[
            v((NP, 32, RW)),
            v((NZ, 32, D)), v((NZ, 32, D)), v((NZ, 32, D)),
            v((D, 512)), v((D, 512)), v((512, D)),
            v((NZ, T, RW)), v((NZ, T, 512)), v((2, NZ, T, 512)),
            v((2, T, 1024)), v((2, NP, T, 1024)), v((NP, T, 128), F32),
            v((NZ, 32, 1024)), v((2, NZ, 32, 1024)), v((2, 128, 1024)), v((128, 1024)),
            v((NZ, 32, 1024)), v((NZ, 32, 1024)),
            v((2, NP * T, 1024)), v((NP * T, 1024)),
            v((NP, T, 1024)), v((NP, T, 1024)), v((4, T, 1024)),
            pltpu.SemaphoreType.DMA((96,)),
            pltpu.SemaphoreType.DMA((96,)),
            pltpu.SemaphoreType.DMA((12,)),
        ],
        compiler_params=pltpu.CompilerParams(
            collective_id=1, has_side_effects=True, vmem_limit_bytes=60 * 1024 * 1024
        ),
        name="ffn",
    )(ret, x, gain, bg, sel, wo, dw, eg, eu, ed)


def selection(route_ids, route_weight):
    p = lax.axis_index("ep") % NP
    y, x = p // 4, p % 4
    flat = route_ids.reshape(-1)
    count = flat.shape[0]
    earlier = jnp.arange(count)[None, :] < jnp.arange(count)[:, None]
    slot = jnp.sum(((flat[:, None] == flat[None, :]) & earlier).astype(jnp.int32), axis=1)
    slot = slot.reshape(route_ids.shape)
    to_z, to_p = route_ids // NP, route_ids % NP
    shift = ((to_p // 4 + 4 - y) % 4) * 4 + (to_p % 4 + 4 - x) % 4
    lane = to_z * 32 + 2 * shift + slot
    widened = route_weight.astype(F32)
    share = widened / jnp.sum(widened, axis=-1, keepdims=True)
    lanes = jnp.arange(128, dtype=jnp.int32)
    shifts = jnp.arange(NP, dtype=jnp.int32)
    total = jnp.zeros((NP, T, 128), F32)
    for k in range(route_ids.shape[1]):
        hit = (shift[None, :, k, None] == shifts[:, None, None]) & (
            lane[None, :, k, None] == lanes[None, None, :]
        )
        total = total + jnp.where(hit, share[None, :, k, None], 0.0)
    return total


def log_decay(head_count):
    spread = jnp.arange(head_count, dtype=F32) * (5.0 / max(head_count - 1, 1))
    return jnp.log1p(-(2.0 ** (-5.0 - spread)))


def on_device(
    inputs, positions, ret_state, norm_mix, w_query, w_key, w_value, w_gate_in, head_gain, w_out,
    norm_ffn, route_ids, route_weight, exp_gate, exp_up, exp_down, dense_gate, dense_up,
    dense_down, branch_gate,
):
    qkvg, wo, dw = project(
        inputs, norm_mix[None, :], w_query, w_key, w_value, w_gate_in,
        w_out.T, dense_gate.T, dense_up.T, dense_down,
    )
    frequency = 10000.0 ** (-jnp.arange(HD // 2, dtype=F32) * 2.0 / HD)
    angles = positions.astype(F32)[:, None] * frequency[None, :]
    cosine, sine = jnp.cos(angles), jnp.sin(angles)
    gamma = lax.dynamic_slice_in_dim(
        jnp.exp(log_decay(HEADS)), lax.axis_index("tp") * LH, LH
    )
    ret, new_state = update(
        qkvg,
        jnp.concatenate([cosine, cosine], axis=-1),
        jnp.concatenate([-sine, sine], axis=-1),
        head_gain[None, :],
        gamma,
        ret_state,
    )
    layer_out = ffn(
        ret, inputs, norm_ffn[None, :], branch_gate[None, :], selection(route_ids, route_weight),
        wo, dw, exp_gate[0], exp_up[0], exp_down[0],
    )
    return (layer_out, new_state)


def solution(mesh):
    in_specs = (
        P("ep", None),
        P("ep"),
        P("ep", "tp", None, None),
        P(),
        P("ep", "tp"),
        P("ep", "tp"),
        P("ep", "tp"),
        P("ep", "tp"),
        P("tp"),
        P("tp", "ep"),
        P(),
        P("ep", None),
        P("ep", None),
        P("ep", None, "tp"),
        P("ep", None, "tp"),
        P("ep", "tp", None),
        P(None, ("ep", "tp")),
        P(None, ("ep", "tp")),
        P(("ep", "tp"), None),
        P(),
    )
    out_specs = (P("ep", None), P("ep", "tp", None, None))
    return jax.shard_map(
        on_device, mesh=mesh, in_specs=in_specs, out_specs=out_specs, check_vma=False
    )
```

time: 341 us -> 111 us (0.33)
  waiting for transfers between devices: 239 us -> 0 us
  Pallas kernels: 0 us -> 100 us
  matrix products: 34.9 us -> 0 us
  starting transfers between devices: 17.9 us -> 0 us
  between operations: 14.1 us -> 0.72 us
  blocking collectives: 13.2 us -> 0 us
  other arithmetic: 15.6 us -> 2.93 us
    all_gather x3 -> x0, waiting for transfers between devices: 175 us -> none  [the longest x1 91.6 us: in_one_piece(): out, at, done = (lax.all_gather(both, axis, axis=dim, tiled=True), 0, [])]
    pallas_call x0 -> x3, Pallas kernels: none -> 100 us  [the longest x1 49.6 us: ffn(): pl.pallas_call(ffn_kernel, out_shape=jax.ShapeDtypeStruct((T, D), BF16),...]
    all_to_all x3 -> x0, waiting for transfers between devices: 63.3 us -> none  [the longest x1 50.4 us: summed_on_arrival(): tiles = lax.all_to_all(split_up(array, dim, size), axis, 0, 0, tiled=True)]
    dot_general x12 -> x0, matrix products: 34.9 us -> none  [the longest x3 7.44 us: on_device(): jnp.dot(normed, weight_rows, preferred_element_type=jnp.float32)]
    all_to_all x3 -> x0, starting transfers between devices: 17.7 us -> none  [the longest x1 6.81 us: summed_on_arrival(): tiles = lax.all_to_all(split_up(array, dim, size), axis, 0, 0, tiled=True)]
    all_to_all x2 -> x0, blocking collectives: 13.2 us -> none  [sent_to_all(): return lax.all_to_all(copies, axis, split_axis=0, concat_axis=0, tiled=True)]
    reduce_sum x10 -> x2, other arithmetic: 4.57 us -> 0.2 us  [the longest x1 0.18 us: selection(): jnp.sum(((flat[:, None] == flat[None, :]) & earlier).astype(jnp.int32), a...]
    broadcast_in_dim x2 -> x5, local copies, waits for them, and re-layouts: 0.05 us -> 3.78 us  [the longest x1 1.29 us: on_device(): norm_mix[None, :]]
  transfers between devices with their start and end apart: 6 -> 0, of which waited for: 5 -> 0; matrix products, arithmetic and copies ran while one was open for 13% -> 0% of each run, Pallas kernels for 0% -> 0%
where the time goes in v1:
time: 111 us; the launch traced here: 110 us
  Pallas kernels  100 us (90%)
  local copies, waits for them, and re-layouts  6.49 us (6%)
  other arithmetic  2.93 us (3%)
    pallas_call x1, Pallas kernels, ffn(): pl.pallas_call(ffn_kernel, out_shape=jax.ShapeDtypeStruct((T, D), BF16),...  49.6 us
    pallas_call x1, Pallas kernels, project(): pl.pallas_call(project_kernel, out_shape=(jax.ShapeDtypeStruct((T, 4 * RW...  40.9 us
    pallas_call x1, Pallas kernels, update(): pl.pallas_call(state_kernel, grid=(T // STEP,), out_shape=(jax.ShapeDtype...  9.88 us

profile of v1, /device:TPU:1, one launch (start us, length us, event | category | flops | bytes accessed | tf_op | source)
XLA Modules:
  0.0 110.5 jit_solution(14075714513983926374)
XLA Ops:
  0.6 1.3 %broadcast_in_dim.63.gain_ref = bf16[1,2048]{1,0:T(2,128)(2,1)} reshape(bf16[2048]{0:T(1024)(128)(2,1)} %param.23) | data formatting | bytes 8192 | tf_op jit(solution)/shard_map/broadcast_in_dim | solution.py:483
  1.9 40.9 %project.1 = (bf16[16,3072]{1,0:T(8,128)(2,1)}, bf16[16,32,768]{2,1,0:T(8,128)(2,1)}, bf16[4,3,32,2048]{3,2,1,0:T(8,128)(2,1)}) custom-call(bf16[16,2048]{1,0:T(8,128)(2,1)} %x_ref.3, bf16[1,2048]{1,0:T(2,128)(2,1)} %broadcast_in_dim.63.gain_ref, bf16[32,768]{1,0:T(8,128)(2,1)} %wq.1, bf16[32,768]{1,0:T(8,128)(2,1)} %wk.1, bf16[32,768]{1,0:T(8,128)(2,1)} %wv.1, ...), custom_call_target="tpu_custom_call" | custom-call | tf_op jit(solution)/shard_map/project/pallas_call | solution.py:171
  42.8 0.7 convert_element_type.9
  43.5 0.1 fusion.15
  43.6 0.7 pad_maximum_fusion
  44.3 1.3 %broadcast_in_dim.64.gain_ref = bf16[1,768]{1,0:T(2,128)(2,1)} reshape(bf16[768]{0:T(1024)(128)(2,1)} %param.28) | data formatting | bytes 3072 | tf_op jit(solution)/shard_map/broadcast_in_dim | solution.py:496
  45.6 0.7 dynamic_slice.3.gamma_ref
  46.2 0.0 copy-start
  46.2 0.0 copy-start.1
  46.2 0.0 copy-start.3
  46.2 0.0 copy-start.2
  46.3 9.9 %state.1 = (bf16[16,768]{1,0:T(8,128)(2,1)}, f32[16,6,128,128]{3,2,1,0:T(8,128)}) custom-call(bf16[16,3072]{1,0:T(8,128)(2,1)} %get-tuple-element.7.q_ref, f32[16,128]{1,0:T(8,128)} %get-tuple-element.29.cos_ref, f32[16,128]{1,0:T(8,128)} %get-tuple-element.30.sin_ref, bf16[1,768]{1,0:T(2,128)(2,1)} %broadcast_in_dim.64.gain_ref, f32[6]{0:T(128)} %dynamic_slice.3.gamma_ref, ...), custom_call_target="tpu_custom_call" | custom-call | tf_op jit(solution)/shard_map/state/pallas_call | solution.py:239
  56.1 0.0 copy-done
  56.1 0.6 broadcast_in_dim.65.gain_ref
  56.7 0.0 copy-done.1
  56.7 0.6 broadcast_in_dim.66.bg_ref
  57.3 0.0 copy-done.3
  57.4 0.0 copy-done.2
  57.4 0.1 copy.32
  57.5 0.1 eq.187
  57.6 0.2 convert_reduce_fusion
  57.7 0.1 reshape.213
  57.9 0.3 slice_reduce_fusion.6
  58.2 0.1 iota_compare_fusion.1
  58.3 0.1 iota_compare_fusion.3
  58.4 0.1 iota_compare_fusion.5
  58.4 0.1 iota_compare_fusion.7
  58.5 0.9 select_add_fusion.sel_ref
  59.4 49.6 %ffn.1 = bf16[16,2048]{1,0:T(8,128)(2,1)} custom-call(bf16[16,768]{1,0:T(8,128)(2,1)} %get-tuple-element.8.ret_ref, bf16[16,2048]{1,0:T(8,128)(2,1)} %x_ref.3, bf16[1,2048]{1,0:T(2,128)(2,1)} %broadcast_in_dim.65.gain_ref, bf16[1,2048]{1,0:T(2,128)(2,1)} %broadcast_in_dim.66.bg_ref, f32[16,16,128]{2,1,0:T(8,128)} %select_add_fusion.sel_ref, ...), custom_call_target="tpu_custom_call" | custom-call | tf_op jit(solution)/shard_map/ffn/pallas_call | solution.py:422
  109.0 1.5 %copy.38 = bf16[16,2048]{1,0:T(8,128)(2,1)} copy(bf16[16,2048]{1,0:T(8,128)(2,1)} %ffn.1) | data formatting | bytes 131072
  (10 shorter events, 0.1 us)
Async XLA Ops:
  46.2 9.9 %copy-start = (bf16[2048]{0:T(1024)(128)(2,1)S(1)}, bf16[2048]{0:T(1024)(128)(2,1)}, u32[]{:S(2)}) copy-start(bf16[2048]{0:T(1024)(128)(2,1)} %param.30) | copy-start | bytes 12292
  46.2 10.5 %copy-start.1 = (bf16[2048]{0:T(1024)(128)(2,1)S(1)}, bf16[2048]{0:T(1024)(128)(2,1)}, u32[]{:S(2)}) copy-start(bf16[2048]{0:T(1024)(128)(2,1)} %param.39) | copy-start | bytes 12292
  46.2 11.1 %copy-start.3 = (bf16[16,4]{0,1:T(4,128)(2,1)S(1)}, bf16[16,4]{0,1:T(4,128)(2,1)}, u32[]{:S(2)}) copy-start(bf16[16,4]{0,1:T(4,128)(2,1)} %param.32) | copy-start | bytes 388
  46.2 11.1 %copy-start.2 = (s32[16,4]{0,1:T(4,128)S(1)}, s32[16,4]{0,1:T(4,128)}, u32[]{:S(2)}) copy-start(s32[16,4]{0,1:T(4,128)} %param.31) | copy-start | bytes 772
